TPU v7x, 32 devices: a whole 2x2x4 slice. The times are simulated.
32 devices in a mesh: gr: 2 (over core), fs: 8 (over z, y), tp: 2 (over x).
Axes of the slice: x: 2, y: 2, z: 4, core: 2. Of those that a mesh axis runs over, the one named last changes fastest.
Arguments:
- tokens: bfloat16 [6144, 2048], P(('gr', 'fs')), may hold values from -6 to 6
- route_ids: int32 [6144, 2], P(('gr', 'fs')), may hold values from 0 to 7, as said below
- route_weights: float32 [6144, 2], P(('gr', 'fs')), may hold values from 0.1 to 1
- norm_gain: float32 [2048], P(('gr', 'fs')), may hold values from 0.1 to 1.9
- gate_weight: float32 [8, 2048, 1024], P(None, ('gr', 'fs'), 'tp'), may hold values from -0.125 to 0.125
- up_weight: float32 [8, 2048, 1024], P(None, ('gr', 'fs'), 'tp'), may hold values from -0.125 to 0.125
- down_weight: float32 [8, 1024, 2048], P(None, ('gr', 'fs'), 'tp'), may hold values from -0.1875 to 0.1875
Outputs:
- gate_new: bfloat16 [8, 2048, 1024], P('fs', None, 'tp')
- up_new: bfloat16 [8, 2048, 1024], P('fs', None, 'tp')
- down_new: bfloat16 [8, 1024, 2048], P('fs', 'tp')
- mixed: bfloat16 [6144, 2048], P(('gr', 'fs'), 'tp')
Inputs may be any that keep to these rules, and one draw needn't show every extreme that they name: `route_ids`: each row names two different experts of one group (expert e belongs to group e // 2); in each device's block of 384 rows every expert is named by exactly 96 rows.
All inputs are finite; a program needn't handle non-finite values.
Results may differ from a plain program's by a relative error of at most 0.015.
Values may be sent and summed in bfloat16 or wider, within the bound.
A program may use at most 64 MiB of HBM per device.

v0:
```python
import functools

import jax
import jax.numpy as jnp
from jax import lax
from jax.experimental import pallas as pl
from jax.experimental.pallas import tpu as pltpu
from jax.sharding import PartitionSpec as P

GROUPS = 4
HEAD = 2
MID = 3
PIECES = 2
RETURN = (3, 1, 2, 0)
BF16 = jnp.bfloat16
MESH = pl.DeviceIdType.MESH


def local(tokens, route_ids, route_weights, norm_gain, gate_weight, up_weight, down_weight):
    gate_folded = (gate_weight * norm_gain[None, :, None]).astype(jnp.bfloat16)
    up_folded = (up_weight * norm_gain[None, :, None]).astype(jnp.bfloat16)
    down_rounded = down_weight.astype(jnp.bfloat16)
    moved = (
        lax.all_to_all(gate_folded, "fs", split_axis=0, concat_axis=1, tiled=True),
        lax.all_to_all(up_folded, "fs", split_axis=0, concat_axis=1, tiled=True),
        lax.all_to_all(down_rounded, "fs", split_axis=0, concat_axis=1, tiled=True),
    )
    gate_new, up_new, down_whole = (
        lax.all_gather(moved[0], "gr", axis=1, tiled=True),
        lax.all_gather(moved[1], "gr", axis=1, tiled=True),
        lax.all_gather(moved[2], "gr", axis=1, tiled=True),
    )
    down_new = lax.all_to_all(down_whole, "tp", split_axis=1, concat_axis=2, tiled=True)
    tok = tokens.shape[0]
    width = tokens.shape[1]
    experts = gate_weight.shape[0]
    cap = 2 * tok // experts
    flat_ids = route_ids.reshape(-1)
    onehot = (flat_ids[:, None] == jnp.arange(experts, dtype=jnp.int32)[None, :]).astype(jnp.int32)
    slot = jnp.sum(jnp.cumsum(onehot, axis=0) * onehot, axis=1) - 1
    position = flat_ids * cap + slot
    source = (
        jnp.zeros((experts * cap,), jnp.int32)
        .at[position]
        .set(jnp.arange(2 * tok, dtype=jnp.int32) // 2)
    )
    widened = tokens.astype(jnp.float32)
    normed = (
        widened * lax.rsqrt(jnp.mean(widened * widened, axis=-1, keepdims=True) + 1e-06)
    ).astype(jnp.bfloat16)
    outgoing = normed[source].reshape(experts, cap, width)
    received = lax.all_to_all(outgoing, "fs", split_axis=0, concat_axis=0, tiled=True)
    senders, count, _ = received.shape
    rows = received.reshape(senders * count, width)
    first = jnp.dot(rows, gate_new[0], preferred_element_type=jnp.float32)
    second = jnp.dot(rows, up_new[0], preferred_element_type=jnp.float32)
    hidden = (jax.nn.silu(first) * second).astype(jnp.bfloat16)
    partial_out = jnp.dot(hidden, down_new[0], preferred_element_type=jnp.float32)
    summed = lax.psum_scatter(
        partial_out.reshape(senders, count, width).astype(jnp.bfloat16),
        "tp",
        scatter_dimension=2,
        tiled=True,
    )
    returned = lax.all_to_all(summed, "fs", split_axis=0, concat_axis=0, tiled=True)
    columns = returned.shape[2]
    route_out = returned.reshape(experts * cap, columns)[position].reshape(tok, 2, columns)
    mixed = jnp.sum(route_weights[:, :, None] * route_out.astype(jnp.float32), axis=1).astype(
        jnp.bfloat16
    )
    return (gate_new, up_new, down_new, mixed)


def place(n_z, n_y):
    f = lax.axis_index("fs")
    return lax.axis_index("gr"), f // n_y, lax.rem(f, n_y), lax.axis_index("tp")


def flip(z, k):
    return (z, z + 1 - 2 * lax.rem(z, 2), lax.rem(z + 2, 4), 3 - z)[k]


def device(c, z, y, x, n_y):
    return {"gr": c, "fs": z * n_y + y, "tp": x}


def greet(peers):
    barrier = pltpu.get_barrier_semaphore()
    for peer in peers:
        pl.semaphore_signal(barrier, inc=1, device_id=peer, device_id_type=MESH)
    pl.semaphore_wait(barrier, len(peers))


def remote(src, dst, send, recv, peer):
    return pltpu.make_async_remote_copy(
        src_ref=src, dst_ref=dst, send_sem=send, recv_sem=recv,
        device_id=peer, device_id_type=MESH,
    )


def sampler(
    n_z, n_y,
    tok_in, ids_in, rw_in, gain_in, gate_in, up_in, down_in,
    gate_out, up_out, down_out, mixed_out,
    wide, narrow, dwide, dnarrow, land, dland, dcross,
    normed, tok_s, rows, rw_s, rw_l, hid, out_s, ry_l, fin, ret,
    ld_sem, w_send, w_recv, f_send, f_recv,
    tz_send, tz_recv, ty_send, ty_recv, tx_send, tx_recv,
    rz_send, rz_recv, ry_send, ry_recv,
    h_send, h_recv, c_send, c_recv, y_send, y_recv, z_send, z_recv, o_sem,
):
    c, z, y, x = place(n_z, n_y)
    me = z * n_y + y
    n_fs = n_z * n_y
    g_rows, d_rows = gate_in.shape[1], down_in.shape[1]
    tok, width = tok_in.shape
    half = width // 2
    cap = tok // GROUPS
    hb = hid.shape[2]
    f32 = jnp.float32
    dev = functools.partial(device, n_y=n_y)
    ks = [(kz, 0) for kz in (1, 3, 2)] + [(kz, 1) for kz in (1, 3, 2, 0)] + [(0, 0)]
    last = len(ks) - 1
    at = []
    for kz, ky in ks:
        pz, py = flip(z, kz), (1 - y if ky else y)
        at.append((pz * n_y + py, dev(c, pz, py, x)))
    other = dev(1 - c, z, y, x)
    x_nbr = dev(c, z, y, 1 - x)
    y_nbr = dev(c, z, 1 - y, x)

    def xcols(i):
        return pl.ds(pl.multiple_of(i * half, half), half)

    def grow(core, f):
        return pl.ds(pl.multiple_of((core * n_fs + f) * g_rows, g_rows), g_rows)

    def drow(core, f):
        return pl.ds(pl.multiple_of((core * n_fs + f) * d_rows, d_rows), d_rows)

    def trow(f):
        return pl.ds(pl.multiple_of(f * cap, cap), cap)

    pair = (gate_in, up_in)
    loads = {}
    for n, (p, _) in enumerate(at):
        for i in range(2):
            loads[n, i] = pltpu.make_async_copy(pair[i].at[p], wide.at[i, n], ld_sem.at[3 * n + i])
            loads[n, i].start()
    for n, (p, _) in enumerate(at):
        loads[n, 2] = pltpu.make_async_copy(down_in.at[p], dwide.at[n], ld_sem.at[3 * n + 2])
        loads[n, 2].start()
    greet([d for _, d in at[:last]] + [other, x_nbr])

    def column(row, count):
        lanes = row.shape[1]
        eye = (lax.broadcasted_iota(jnp.int32, (count, lanes), 0)
               == lax.broadcasted_iota(jnp.int32, (count, lanes), 1))
        return jnp.sum(jnp.where(eye, row, 0.0), axis=1, keepdims=True)

    gain = column(gain_in[...], g_rows)
    arrive = {}
    onward = {}

    def fold(n):
        p, peer = at[n]
        for i in range(2):
            loads[n, i].wait()
            value = (wide[i, n] * gain).astype(BF16)
            if n == last:
                land[i, grow(c, me)] = value
                block = land.at[i, grow(c, me)]
                onward[n, i] = remote(block, block, f_send.at[3 * n + i], f_recv.at[3 * n + i], other)
                onward[n, i].start()
            else:
                narrow[i, n] = value
                cp = remote(narrow.at[i, n], land.at[i, grow(c, me)],
                            w_send.at[3 * n + i], w_recv.at[3 * n + i], peer)
                cp.start()
                arrive[n, i] = cp

    for n in range(HEAD):
        fold(n)

    def norm_rows(i, carry):
        r = pl.ds(pl.multiple_of(i * cap, cap), cap)
        v = tok_in[r, :].astype(f32)
        scale = lax.rsqrt(jnp.mean(v * v, axis=-1, keepdims=True) + 1e-06)
        normed[r, :] = (tok_in[r, xcols(x)].astype(f32) * scale).astype(BF16)
        return carry

    lax.fori_loop(0, GROUPS, norm_rows, 0)
    epg = gate_in.shape[0] // GROUPS
    low = ids_in[0:1, :]
    group = jnp.zeros_like(low)
    for g in range(1, GROUPS):
        group += (low >= g * epg).astype(jnp.int32)
    ahead = low == group * epg
    w_a, w_b = rw_in[0:1, :], rw_in[1:2, :]
    sub = lax.broadcasted_iota(jnp.int32, (8, tok), 0)
    w_of = jnp.where(sub == 0, jnp.where(ahead, w_a, w_b),
                     jnp.where(sub == 1, jnp.where(ahead, w_b, w_a), 0.0))
    onehot = (lax.broadcasted_iota(jnp.int32, (8, tok), 0) == group).astype(f32)
    upto = (lax.broadcasted_iota(jnp.int32, (tok, tok), 0)
            <= lax.broadcasted_iota(jnp.int32, (tok, tok), 1)).astype(BF16)
    count = jnp.dot(onehot.astype(BF16), upto, preferred_element_type=f32)
    slot = jnp.sum(onehot * count, axis=0, keepdims=True).astype(jnp.int32) - 1
    position = group * cap + slot

    def picked(g):
        return lax.broadcasted_iota(jnp.int32, (cap, tok), 0) + g * cap == position

    tz, rz, ty, tx, ry = {}, {}, {}, {}, {}
    for kz in (1, 3, 2, 0):
        g = flip(z, kz)
        pick = picked(g)
        block = jnp.dot(pick.astype(BF16), normed[...], preferred_element_type=f32).astype(BF16)
        w_row = lax.dot_general(w_of, pick.astype(f32), (((1,), (1,)), ((), ())),
                                precision=lax.Precision.HIGHEST, preferred_element_type=f32)
        if kz:
            tok_s[kz] = block
            rw_s[kz, :, :cap] = w_row
            peer = dev(c, g, y, x)
            tz[kz] = remote(tok_s.at[kz], rows.at[trow(me), xcols(x)],
                            tz_send.at[kz], tz_recv.at[kz], peer)
            tz[kz].start()
            rz[kz] = remote(rw_s.at[kz], rw_l.at[me], rz_send.at[kz], rz_recv.at[kz], peer)
            rz[kz].start()
        else:
            rows[trow(me), xcols(x)] = block
            rw_l[me, :, :cap] = w_row

    def pass_on(kz):
        src = flip(z, kz) * n_y + y
        block = rows.at[trow(src), xcols(x)]
        ty[kz] = remote(block, block, ty_send.at[kz], ty_recv.at[kz], y_nbr)
        ty[kz].start()
        tx[kz] = remote(block, block, tx_send.at[kz], tx_recv.at[kz], x_nbr)
        tx[kz].start()
        ry[kz] = remote(rw_l.at[src], rw_l.at[src], ry_send.at[kz], ry_recv.at[kz], y_nbr)
        ry[kz].start()

    pass_on(0)
    for n in list(range(HEAD, MID)) + [last]:
        fold(n)
    for kz in (1, 3, 2):
        tz[kz].wait_recv()
        rz[kz].wait_recv()
        pass_on(kz)
    for n in range(MID, last):
        fold(n)
    for n, (p, peer) in enumerate(at):
        loads[n, 2].wait()
        value = dwide[n].astype(BF16)
        if n == last:
            dland[drow(c, me)] = value
            block = dland.at[drow(c, me)]
            onward[n, 2] = remote(block, block, f_send.at[3 * n + 2], f_recv.at[3 * n + 2], other)
            onward[n, 2].start()
        else:
            dnarrow[n] = value
            arrive[n, 2] = remote(dnarrow.at[n], dland.at[drow(c, me)],
                                  w_send.at[3 * n + 2], w_recv.at[3 * n + 2], peer)
            arrive[n, 2].start()

    for kz in (0, 1, 3, 2):
        ty[kz].wait_recv()
        block = rows.at[trow(flip(z, kz) * n_y + 1 - y), xcols(x)]
        tx[4 + kz] = remote(block, block, tx_send.at[4 + kz], tx_recv.at[4 + kz], x_nbr)
        tx[4 + kz].start()

    order = sorted(range(last), key=lambda n: ks[n])
    for n in order:
        for i in range(2):
            arrive[n, i].wait_recv()
            block = land.at[i, grow(c, at[n][0])]
            onward[n, i] = remote(block, block, f_send.at[3 * n + i], f_recv.at[3 * n + i], other)
            onward[n, i].start()
    for cp in list(tx.values()) + list(ry.values()):
        cp.wait_recv()
    for n in [last] + order:
        for i in range(2):
            onward[n, i].wait_recv()
    outs = []
    for i, out in enumerate((gate_out, up_out)):
        cp = pltpu.make_async_copy(land.at[i], out.at[0], o_sem.at[i])
        cp.start()
        outs.append(cp)

    m = n_y * cap
    q = min(hb, 256)
    hsend = []
    for n, kz in enumerate(RETURN):
        r = pl.ds(pl.multiple_of(flip(z, kz) * m, m), m)

        def units(i, carry):
            s = pl.ds(pl.multiple_of(i * q, q), q)
            a = jnp.dot(rows[r, :], land[0, :, s], preferred_element_type=f32)
            b = jnp.dot(rows[r, :], land[1, :, s], preferred_element_type=f32)
            hid[x, r, s] = (a / (1.0 + jnp.exp(-a)) * b).astype(BF16)
            return carry

        lax.fori_loop(0, hb // q, units, 0)
        cp = remote(hid.at[x, r], hid.at[x, r], h_send.at[n], h_recv.at[n], x_nbr)
        cp.start()
        hsend.append(cp)

    for n in order:
        arrive[n, 2].wait_recv()
        block = dland.at[drow(c, at[n][0])]
        onward[n, 2] = remote(block, block, f_send.at[3 * n + 2], f_recv.at[3 * n + 2], other)
        onward[n, 2].start()
    for n in [last] + order:
        onward[n, 2].wait_recv()
    part = hb // 2
    mine = pl.ds(pl.multiple_of(c * part, part), part)
    cross = remote(
        dland.at[pl.ds(pl.multiple_of((1 - x) * hb + c * part, part), part)],
        dcross.at[mine], c_send.at[0], c_recv.at[0], x_nbr)
    cross.start()
    cp = pltpu.make_async_copy(
        dland.at[pl.ds(pl.multiple_of(x * hb, hb), hb)], down_out.at[0, :, xcols(x)], o_sem.at[2])
    cp.start()
    outs.append(cp)

    piece = half // PIECES
    ysend = {}
    zsend = []

    def give_back(n):
        kz = RETURN[n]
        for h in range(PIECES):
            d = pl.ds(h * piece, piece)
            ysend[n, h].wait_recv()
            total = (out_s[n, 1, :, d].astype(f32) + ry_l[n, :, d].astype(f32)).astype(BF16)
            if kz:
                i = n * PIECES + h
                fin[n, :, d] = total
                cp = remote(fin.at[n, :, d], ret.at[trow(z), d], z_send.at[i], z_recv.at[i],
                            dev(c, flip(z, kz), y, x))
                cp.start()
                zsend.append(cp)
            else:
                ret[trow(z), d] = total

    for n, kz in enumerate(RETURN):
        zs = flip(z, kz)
        hsend[n].wait_recv()
        for step in range(2):
            s = 1 - y if step == 0 else y
            f = zs * n_y + s
            w = jnp.where(y == 0, rw_l[f, 0:1, :], rw_l[f, 1:2, :])
            lane = lax.broadcasted_iota(jnp.int32, w.shape, 1)
            w = column(jnp.where(lane < cap, w, 0.0), cap)
            for h in range(PIECES):
                d = pl.ds(h * piece, piece)
                acc = jnp.dot(hid[0, trow(f)], dland[:hb, d], preferred_element_type=f32)
                acc += jnp.dot(hid[1, trow(f)], dland[hb:, d], preferred_element_type=f32)
                out_s[n, step, :, d] = (acc * w).astype(BF16)
                if step == 0:
                    i = n * PIECES + h
                    cp = remote(out_s.at[n, 0, :, d], ry_l.at[n, :, d],
                                y_send.at[i], y_recv.at[i], y_nbr)
                    cp.start()
                    ysend[n, h] = cp
        if n:
            give_back(n - 1)
    give_back(len(RETURN) - 1)

    cross.wait_recv()
    over = remote(dcross.at[mine], dcross.at[mine], c_send.at[1], c_recv.at[1], other)
    over.start()
    for cp in zsend:
        cp.wait_recv()
    everyone = (lax.broadcasted_iota(jnp.int32, (tok, tok), 0) == position).astype(BF16)
    mixed_out[...] = lax.dot_general(
        everyone, ret[...], (((0,), (0,)), ((), ())), preferred_element_type=f32).astype(BF16)
    over.wait_recv()
    cp = pltpu.make_async_copy(dcross, down_out.at[0, :, xcols(1 - x)], o_sem.at[3])
    cp.start()
    outs.append(cp)
    for cp in outs:
        cp.wait()
    for group_of in (arrive, onward, tz, rz, ty, tx, ry):
        for cp in group_of.values():
            cp.wait_send()
    for cp in hsend + list(ysend.values()) + zsend + [cross, over]:
        cp.wait_send()


def paired(n_z, n_y, tokens, route_ids, route_weights, norm_gain, gate_weight, up_weight, down_weight):
    tok, width = tokens.shape
    cap = tok // GROUPS
    half = width // lax.axis_size("tp")
    n_fs = n_z * n_y
    d_rows, d_cols = down_weight.shape[1:]
    g_rows, g_cols = gate_weight.shape[1:]
    f32 = jnp.float32

    hbm = pl.BlockSpec(memory_space=pl.ANY)
    vmem = pl.BlockSpec(memory_space=pltpu.VMEM)
    dma = pltpu.SemaphoreType.DMA
    lanes = -(-cap // 128) * 128
    gate_new, up_new, down_new, mixed = pl.pallas_call(
        functools.partial(sampler, n_z, n_y),
        out_shape=(
            jax.ShapeDtypeStruct((1, 2 * n_fs * g_rows, g_cols), BF16),
            jax.ShapeDtypeStruct((1, 2 * n_fs * g_rows, g_cols), BF16),
            jax.ShapeDtypeStruct((1, n_fs * d_rows, 2 * d_cols), BF16),
            jax.ShapeDtypeStruct((tok, half), BF16),
        ),
        in_specs=[vmem] * 4 + [pl.BlockSpec(memory_space=pltpu.HBM)] * 3,
        out_specs=(hbm, hbm, hbm, vmem),
        scratch_shapes=[
            pltpu.VMEM((2, n_fs, g_rows, g_cols), f32),
            pltpu.VMEM((2, n_fs - 1, g_rows, g_cols), BF16),
            pltpu.VMEM((n_fs, d_rows, d_cols), f32),
            pltpu.VMEM((n_fs - 1, d_rows, d_cols), BF16),
            pltpu.VMEM((2, 2 * n_fs * g_rows, g_cols), BF16),
            pltpu.VMEM((2 * n_fs * d_rows, d_cols), BF16),
            pltpu.VMEM((n_fs * d_rows, d_cols), BF16),
            pltpu.VMEM((tok, half), BF16),
            pltpu.VMEM((4, cap, half), BF16),
            pltpu.VMEM((n_fs * cap, width), BF16),
            pltpu.VMEM((4, 8, lanes), f32),
            pltpu.VMEM((n_fs, 8, lanes), f32),
            pltpu.VMEM((2, n_fs * cap, n_fs * d_rows), BF16),
            pltpu.VMEM((4, 2, cap, half), BF16),
            pltpu.VMEM((4, cap, half), BF16),
            pltpu.VMEM((4, cap, half), BF16),
            pltpu.VMEM((GROUPS * cap, half), BF16),
            dma((3 * n_fs,)),
            dma((3 * n_fs,)), dma((3 * n_fs,)), dma((3 * n_fs,)), dma((3 * n_fs,)),
            dma((4,)), dma((4,)), dma((4,)), dma((4,)), dma((8,)), dma((8,)),
            dma((4,)), dma((4,)), dma((4,)), dma((4,)),
            dma((4,)), dma((4,)), dma((2,)), dma((2,)), dma((4 * PIECES,)), dma((4 * PIECES,)),
            dma((4 * PIECES,)), dma((4 * PIECES,)), dma((4,)),
        ],
        compiler_params=pltpu.CompilerParams(
            collective_id=0, has_side_effects=True, vmem_limit_bytes=44 * 1024 * 1024),
    )(tokens, route_ids.T, route_weights.T, norm_gain.reshape(1, g_rows), gate_weight, up_weight, down_weight)
    return gate_new, up_new, down_new, mixed


def solution(mesh):
    placed = (
        P(("gr", "fs"), None),
        P(("gr", "fs"), None),
        P(("gr", "fs"), None),
        P(("gr", "fs")),
        P(None, ("gr", "fs"), "tp"),
        P(None, ("gr", "fs"), "tp"),
        P(None, ("gr", "fs"), "tp"),
    )
    n_fs = mesh.shape["fs"]

    def body(*args):
        experts = args[4].shape[0]
        if experts == n_fs == 2 * GROUPS and mesh.shape["gr"] == mesh.shape["tp"] == 2:
            return paired(GROUPS, 2, *args)
        return local(*args)

    return jax.shard_map(
        body,
        mesh=mesh,
        in_specs=placed,
        out_specs=(
            P("fs", None, "tp"),
            P("fs", None, "tp"),
            P("fs", "tp", None),
            P(("gr", "fs"), "tp"),
        ),
        check_vma=False,
    )
```

profile of v0, /device:TPU:0, one launch (start us, length us, event | category | flops | bytes accessed | tf_op | source)
XLA Modules:
  0.0 127.0 jit_solution(7585519102028961861)
XLA Ops:
  0.6 0.0 copy-start
  0.6 1.4 %copy-done = bf16[384,2048]{1,0:T(8,128)(2,1)S(1)} copy-done((bf16[384,2048]{1,0:T(8,128)(2,1)S(1)}, bf16[384,2048]{1,0:T(8,128)(2,1)}, u32[]{:S(2)}) %copy-start) | copy-done | bytes 1572888
  2.0 0.0 copy-start.1
  2.0 0.7 copy-done.1
  2.7 0.0 copy-start.2
  2.7 0.7 copy-done.2
  3.4 0.0 copy-start.3
  3.4 0.7 copy-done.3
  4.1 118.1 %shard_map.102 = (bf16[1,2048,512]{2,1,0:T(8,128)(2,1)S(1)}, bf16[1,2048,512]{2,1,0:T(8,128)(2,1)S(1)}, bf16[1,512,2048]{2,1,0:T(8,128)(2,1)S(1)}, bf16[384,1024]{1,0:T(8,128)(2,1)S(1)}) custom-call(bf16[384,2048]{1,0:T(8,128)(2,1)S(1)} %copy-done, s32[2,384]{1,0:T(2,128)S(1)} %bitcast.3, f32[2,384]{1,0:T(2,128)S(1)} %bitcast.4, f32[1,128]{1,0:T(1,128)S(1)} %bitcast.5, ...), custom_call_target="tpu_custom_call" | custom-call | tf_op jit(solution)/shard_map/pallas_call | solution.py:404
  122.2 1.3 %copy.15 = bf16[1,2048,512]{2,1,0:T(8,128)(2,1)} copy(bf16[1,2048,512]{2,1,0:T(8,128)(2,1)S(1)} %get-tuple-element.8) | data formatting | bytes 4194304
  123.5 1.3 %copy.16 = bf16[1,2048,512]{2,1,0:T(8,128)(2,1)} copy(bf16[1,2048,512]{2,1,0:T(8,128)(2,1)S(1)} %get-tuple-element.9) | data formatting | bytes 4194304
  124.8 1.3 %copy.17 = bf16[1,512,2048]{2,1,0:T(8,128)(2,1)} copy(bf16[1,512,2048]{2,1,0:T(8,128)(2,1)S(1)} %get-tuple-element.10) | data formatting | bytes 4194304
  126.2 0.9 copy.18
Async XLA Ops:
  0.6 1.4 %copy-start = (bf16[384,2048]{1,0:T(8,128)(2,1)S(1)}, bf16[384,2048]{1,0:T(8,128)(2,1)}, u32[]{:S(2)}) copy-start(bf16[384,2048]{1,0:T(8,128)(2,1)} %tok_in.1) | copy-start | bytes 4718596
  2.0 0.7 copy-start.1
  2.7 0.7 copy-start.2
  3.4 0.7 copy-start.3
where the time goes:
time: 127 us
  Pallas kernels  118 us (93%)
  local copies, waits for them, and re-layouts  8.26 us (7%)
    pallas_call x1, Pallas kernels, paired(): pl.pallas_call(functools.partial(sampler, n_z, n_y), out_shape=(jax.Shape...  118 us
    unnamed x12, local copies, waits for them, and re-layouts  8.26 us

commit v1 on v0

v1 whole, which is shorter than its diff:
```python
import functools

import jax
import jax.numpy as jnp
from jax import lax
from jax.experimental import pallas as pl
from jax.experimental.pallas import tpu as pltpu
from jax.sharding import PartitionSpec as P

GROUPS = 4
HEAD = 2
HALVES = 2
RETURN = (3, 2, 1, 0)
BF16 = jnp.bfloat16
MESH = pl.DeviceIdType.MESH


def local(tokens, route_ids, route_weights, norm_gain, gate_weight, up_weight, down_weight):
    gate_folded = (gate_weight * norm_gain[None, :, None]).astype(jnp.bfloat16)
    up_folded = (up_weight * norm_gain[None, :, None]).astype(jnp.bfloat16)
    down_rounded = down_weight.astype(jnp.bfloat16)
    moved = (
        lax.all_to_all(gate_folded, "fs", split_axis=0, concat_axis=1, tiled=True),
        lax.all_to_all(up_folded, "fs", split_axis=0, concat_axis=1, tiled=True),
        lax.all_to_all(down_rounded, "fs", split_axis=0, concat_axis=1, tiled=True),
    )
    gate_new, up_new, down_whole = (
        lax.all_gather(moved[0], "gr", axis=1, tiled=True),
        lax.all_gather(moved[1], "gr", axis=1, tiled=True),
        lax.all_gather(moved[2], "gr", axis=1, tiled=True),
    )
    down_new = lax.all_to_all(down_whole, "tp", split_axis=1, concat_axis=2, tiled=True)
    tok = tokens.shape[0]
    width = tokens.shape[1]
    experts = gate_weight.shape[0]
    cap = 2 * tok // experts
    flat_ids = route_ids.reshape(-1)
    onehot = (flat_ids[:, None] == jnp.arange(experts, dtype=jnp.int32)[None, :]).astype(jnp.int32)
    slot = jnp.sum(jnp.cumsum(onehot, axis=0) * onehot, axis=1) - 1
    position = flat_ids * cap + slot
    source = (
        jnp.zeros((experts * cap,), jnp.int32)
        .at[position]
        .set(jnp.arange(2 * tok, dtype=jnp.int32) // 2)
    )
    widened = tokens.astype(jnp.float32)
    normed = (
        widened * lax.rsqrt(jnp.mean(widened * widened, axis=-1, keepdims=True) + 1e-06)
    ).astype(jnp.bfloat16)
    outgoing = normed[source].reshape(experts, cap, width)
    received = lax.all_to_all(outgoing, "fs", split_axis=0, concat_axis=0, tiled=True)
    senders, count, _ = received.shape
    rows = received.reshape(senders * count, width)
    first = jnp.dot(rows, gate_new[0], preferred_element_type=jnp.float32)
    second = jnp.dot(rows, up_new[0], preferred_element_type=jnp.float32)
    hidden = (jax.nn.silu(first) * second).astype(jnp.bfloat16)
    partial_out = jnp.dot(hidden, down_new[0], preferred_element_type=jnp.float32)
    summed = lax.psum_scatter(
        partial_out.reshape(senders, count, width).astype(jnp.bfloat16),
        "tp",
        scatter_dimension=2,
        tiled=True,
    )
    returned = lax.all_to_all(summed, "fs", split_axis=0, concat_axis=0, tiled=True)
    columns = returned.shape[2]
    route_out = returned.reshape(experts * cap, columns)[position].reshape(tok, 2, columns)
    mixed = jnp.sum(route_weights[:, :, None] * route_out.astype(jnp.float32), axis=1).astype(
        jnp.bfloat16
    )
    return (gate_new, up_new, down_new, mixed)


def place(n_z, n_y):
    f = lax.axis_index("fs")
    return lax.axis_index("gr"), f // n_y, lax.rem(f, n_y), lax.axis_index("tp")


def flip(z, k):
    return (z, z + 1 - 2 * lax.rem(z, 2), lax.rem(z + 2, 4), 3 - z)[k]


def device(c, z, y, x, n_y):
    return {"gr": c, "fs": z * n_y + y, "tp": x}


def greet(peers):
    barrier = pltpu.get_barrier_semaphore()
    for peer in peers:
        pl.semaphore_signal(barrier, inc=1, device_id=peer, device_id_type=MESH)
    return lambda: pl.semaphore_wait(barrier, len(peers))


def remote(src, dst, send, recv, peer):
    return pltpu.make_async_remote_copy(
        src_ref=src, dst_ref=dst, send_sem=send, recv_sem=recv,
        device_id=peer, device_id_type=MESH,
    )


def landed(ref, sem):
    pltpu.make_async_copy(ref, ref, sem).wait()


def sampler(
    n_z, n_y,
    tok_hbm, ids_hbm, rw_hbm, gain_hbm, gate_in, up_in, down_in,
    land, dland, dcross, ret, spot,
    tok_in, ids_in, rw_in, gain_in, wide, narrow, dwide, dnarrow,
    normed, tok_s, rows, rw_s, rw_l, hid, out_s, ry_l, fin,
    in_sem, ld_sem, dl_sem, w_send, w_recv, f_send, f_recv,
    tz_send, tz_recv, ty_send, ty_recv, tx_send, tx_recv,
    rz_send, rz_recv, ry_send, ry_recv,
    h_send, h_recv, c_send, c_recv, y_send, y_recv, z_send, z_recv,
):
    c, z, y, x = place(n_z, n_y)
    me = z * n_y + y
    n_fs = n_z * n_y
    g_rows, d_rows = gate_in.shape[1], down_in.shape[1]
    tok, width = tok_in.shape
    half = width // 2
    cap = tok // GROUPS
    hb = n_fs * d_rows
    q = hb // HALVES
    piece = half // HALVES
    f32 = jnp.float32
    dev = functools.partial(device, n_y=n_y)
    ks = [(kz, 0) for kz in (3, 2, 1)] + [(kz, 1) for kz in (3, 2, 1, 0)] + [(0, 0)]
    last = len(ks) - 1
    at = []
    for kz, ky in ks:
        pz, py = flip(z, kz), (1 - y if ky else y)
        at.append((pz * n_y + py, dev(c, pz, py, x)))
    other = dev(1 - c, z, y, x)
    x_nbr = dev(c, z, y, 1 - x)
    y_nbr = dev(c, z, 1 - y, x)

    def xcols(i):
        return pl.ds(pl.multiple_of(i * half, half), half)

    def grow(core, f):
        return pl.ds(pl.multiple_of((core * n_fs + f) * g_rows, g_rows), g_rows)

    def drow(core, f):
        return pl.ds(pl.multiple_of((core * n_fs + f) * d_rows, d_rows), d_rows)

    def core_rows(core, count):
        return pl.ds(pl.multiple_of(core * n_fs * count, n_fs * count), n_fs * count)

    def trow(f):
        return pl.ds(pl.multiple_of(f * cap, cap), cap)

    met = greet([d for _, d in at[:last]] + [other, x_nbr])
    small = []

    def fetch(src, dst):
        cp = pltpu.make_async_copy(src, dst, in_sem.at[len(small)])
        cp.start()
        small.append(cp)

    fetch(gain_hbm, gain_in)
    loads = {}

    def load(n):
        for i, ref in enumerate((gate_in, up_in)):
            pltpu.make_async_copy(ref.at[at[n][0]], wide.at[n, i], ld_sem.at[n]).start()

    for n in range(HEAD):
        load(n)
    fetch(tok_hbm, tok_in)
    fetch(ids_hbm, ids_in)
    fetch(rw_hbm, rw_in)
    for n in range(HEAD, last + 1):
        load(n)
    for n, (p, _) in enumerate(at):
        pltpu.make_async_copy(down_in.at[p], dwide.at[n], dl_sem.at[0]).start()

    def column(row, count):
        lanes = row.shape[1]
        eye = (lax.broadcasted_iota(jnp.int32, (count, lanes), 0)
               == lax.broadcasted_iota(jnp.int32, (count, lanes), 1))
        return jnp.sum(jnp.where(eye, row, 0.0), axis=1, keepdims=True)

    small[0].wait()
    gain = column(gain_in[...], g_rows)

    def fold(n):
        landed(wide.at[n], ld_sem.at[n])
        for i in range(2):
            value = (wide[n, i] * gain).astype(BF16)
            for a in range(HALVES):
                part = value[:, a * q:(a + 1) * q]
                if n == last:
                    land[a, i, grow(c, me), :] = part
                else:
                    narrow[n, a, i] = part

    arrive = {}
    onward = {}

    def forward(n, a):
        block = land.at[a, :, grow(c, at[n][0]), :]
        onward[n, a] = remote(block, block, f_send.at[0], f_recv.at[a], other)
        onward[n, a].start()

    def spread(n, a):
        if n == last:
            forward(n, a)
        else:
            arrive[n, a] = remote(narrow.at[n, a], land.at[a, :, grow(c, me), :],
                                  w_send.at[0], w_recv.at[a, n], at[n][1])
            arrive[n, a].start()

    for n in range(HEAD):
        fold(n)
    met()
    for n in range(HEAD):
        spread(n, 0)

    for cp in small[1:]:
        cp.wait()

    def norm_rows(i, carry):
        r = pl.ds(pl.multiple_of(i * cap, cap), cap)
        v = tok_in[r, :].astype(f32)
        scale = lax.rsqrt(jnp.mean(v * v, axis=-1, keepdims=True) + 1e-06)
        normed[r, :] = (tok_in[r, xcols(x)].astype(f32) * scale).astype(BF16)
        return carry

    lax.fori_loop(0, GROUPS, norm_rows, 0)
    epg = gate_in.shape[0] // GROUPS
    low = ids_in[0:1, :]
    group = jnp.zeros_like(low)
    for g in range(1, GROUPS):
        group += (low >= g * epg).astype(jnp.int32)
    ahead = low == group * epg
    w_a, w_b = rw_in[0:1, :], rw_in[1:2, :]
    sub = lax.broadcasted_iota(jnp.int32, (8, tok), 0)
    w_of = jnp.where(sub == 0, jnp.where(ahead, w_a, w_b),
                     jnp.where(sub == 1, jnp.where(ahead, w_b, w_a), 0.0))
    onehot = (lax.broadcasted_iota(jnp.int32, (8, tok), 0) == group).astype(f32)
    upto = (lax.broadcasted_iota(jnp.int32, (tok, tok), 0)
            <= lax.broadcasted_iota(jnp.int32, (tok, tok), 1)).astype(BF16)
    count = jnp.dot(onehot.astype(BF16), upto, preferred_element_type=f32)
    slot = jnp.sum(onehot * count, axis=0, keepdims=True).astype(jnp.int32) - 1
    position = group * cap + slot
    spot[...] = jnp.broadcast_to(position, spot.shape)

    def picked(g):
        return lax.broadcasted_iota(jnp.int32, (cap, tok), 0) + g * cap == position

    tz, rz, ty, tx, ry = {}, {}, {}, {}, {}
    for kz in (3, 2, 1, 0):
        g = flip(z, kz)
        pick = picked(g)
        block = jnp.dot(pick.astype(BF16), normed[...], preferred_element_type=f32).astype(BF16)
        w_row = lax.dot_general(w_of, pick.astype(f32), (((1,), (1,)), ((), ())),
                                precision=lax.Precision.HIGHEST, preferred_element_type=f32)
        if kz:
            tok_s[kz - 1] = block
            rw_s[kz - 1, :, :cap] = w_row
            peer = dev(c, g, y, x)
            tz[kz] = remote(tok_s.at[kz - 1], rows.at[trow(me), xcols(x)],
                            tz_send.at[0], tz_recv.at[kz - 1], peer)
            tz[kz].start()
            rz[kz] = remote(rw_s.at[kz - 1], rw_l.at[y, z], rz_send.at[0], rz_recv.at[kz - 1], peer)
            rz[kz].start()
        else:
            rows[trow(me), xcols(x)] = block
            rw_l[y, z, :, :cap] = w_row

    def pass_x(f):
        block = rows.at[trow(f), xcols(x)]
        tx[len(tx)] = remote(block, block, tx_send.at[0], tx_recv.at[0], x_nbr)
        tx[len(tx) - 1].start()

    def pass_on(kz):
        zs = flip(z, kz)
        src = zs * n_y + y
        block = rows.at[trow(src), xcols(x)]
        ty[kz] = remote(block, block, ty_send.at[0], ty_recv.at[kz], y_nbr)
        ty[kz].start()
        pass_x(src)
        ry[kz] = remote(rw_l.at[y, zs], rw_l.at[y, zs], ry_send.at[0], ry_recv.at[0], y_nbr)
        ry[kz].start()

    pass_on(0)
    for n in range(HEAD, last + 1):
        fold(n)
        spread(n, 0)
    for n in range(last + 1):
        spread(n, 1)

    landed(dwide, dl_sem.at[0])

    def dforward(n, h):
        block = dland.at[h, drow(c, at[n][0])]
        onward[n, 2 + h] = remote(block, block, f_send.at[1], f_recv.at[2 + h], other)
        onward[n, 2 + h].start()

    for h in range(HALVES):
        for n in range(last + 1):
            value = dwide[n, :, h * piece:(h + 1) * piece].astype(BF16)
            if n == last:
                dland[h, drow(c, me)] = value
                dforward(n, h)
            else:
                dnarrow[h, n] = value
                arrive[n, 2 + h] = remote(dnarrow.at[h, n], dland.at[h, drow(c, me)],
                                          w_send.at[1], w_recv.at[2 + h, n], at[n][1])
                arrive[n, 2 + h].start()

    for kz in (1, 3, 2):
        tz[kz].wait_recv()
        rz[kz].wait_recv()
        pass_on(kz)
    for kz in (0, 1, 3, 2):
        ty[kz].wait_recv()
        pass_x(flip(z, kz) * n_y + 1 - y)

    order = sorted(range(last), key=lambda n: ks[n])

    def gather(a):
        for n in order:
            arrive[n, a].wait_recv()
            forward(n, a)
        if a == 0:
            landed(rows.at[:, xcols(1 - x)], tx_recv.at[0])
            landed(rw_l.at[1 - y], ry_recv.at[0])
        landed(land.at[a, :, core_rows(1 - c, g_rows), :], f_recv.at[a])

    m = n_y * cap
    hsend = {}
    for a in range(HALVES):
        gather(a)
        for n, kz in enumerate(RETURN):
            r = pl.ds(pl.multiple_of(flip(z, kz) * m, m), m)
            v = jnp.dot(rows[r, :], land[a, 0], preferred_element_type=f32)
            w = jnp.dot(rows[r, :], land[a, 1], preferred_element_type=f32)
            hid[x, a, r, :] = (v / (1.0 + jnp.exp(-v)) * w).astype(BF16)
            cp = remote(hid.at[x, a, r], hid.at[x, a, r], h_send.at[0], h_recv.at[a, n], x_nbr)
            cp.start()
            hsend[a, n] = cp

    part = hb // 2
    mine = pl.ds(pl.multiple_of(c * part, part), part)
    cross = []
    ysend = {}
    zsend = {}

    def give_back(n, h):
        kz = RETURN[n]
        ysend[n, h].wait_recv()
        total = (out_s[h, n, 1].astype(f32) + ry_l[h, n].astype(f32)).astype(BF16)
        d = pl.ds(h * piece, piece)
        if kz:
            fin[h, n] = total
            zsend[n, h] = remote(fin.at[h, n], ret.at[trow(z), d], z_send.at[0], z_recv.at[h],
                                 dev(c, flip(z, kz), y, x))
            zsend[n, h].start()
        else:
            ret[trow(z), d] = total

    for h in range(HALVES):
        for n in order:
            arrive[n, 2 + h].wait_recv()
            dforward(n, h)
        landed(dland.at[h, core_rows(1 - c, d_rows)], f_recv.at[2 + h])
        cp = remote(dland.at[h, pl.ds(pl.multiple_of((1 - x) * hb + c * part, part), part)],
                    dcross.at[h, mine], c_send.at[0], c_recv.at[h], x_nbr)
        for n, kz in enumerate(RETURN):
            zs = flip(z, kz)
            if h == 0:
                for a in range(HALVES):
                    hsend[a, n].wait_recv()
            for step in range(2):
                s = 1 - y if step == 0 else y
                f = zs * n_y + s
                w = jnp.where(y == 0, rw_l[s, zs, 0:1, :], rw_l[s, zs, 1:2, :])
                lane = lax.broadcasted_iota(jnp.int32, w.shape, 1)
                w = column(jnp.where(lane < cap, w, 0.0), cap)
                acc = jnp.zeros((cap, piece), f32)
                for i in range(2):
                    for a in range(HALVES):
                        acc += jnp.dot(hid[i, a, trow(f)], dland[h, pl.ds(i * hb + a * q, q)],
                                       preferred_element_type=f32)
                out_s[h, n, step] = (acc * w).astype(BF16)
                if step == 0:
                    ysend[n, h] = remote(out_s.at[h, n, 0], ry_l.at[h, n],
                                         y_send.at[0], y_recv.at[h, n], y_nbr)
                    ysend[n, h].start()
            if n:
                give_back(n - 1, h)
        cp.start()
        cross.append(cp)
        give_back(len(RETURN) - 1, h)

    over = []
    for h in range(HALVES):
        cross[h].wait_recv()
        block = dcross.at[h, mine]
        cp = remote(block, block, c_send.at[1], c_recv.at[2 + h], other)
        cp.start()
        over.append(cp)
    for h in range(HALVES):
        landed(fin.at[h, pl.ds(0, GROUPS - 1)], z_recv.at[h])
    for cp in over:
        cp.wait_recv()
    landed(narrow, w_send.at[0])
    landed(dnarrow, w_send.at[1])
    landed(land.at[:, :, core_rows(c, g_rows), :], f_send.at[0])
    landed(dland.at[:, core_rows(c, d_rows)], f_send.at[1])
    landed(tok_s, tz_send.at[0])
    landed(rw_s, rz_send.at[0])
    landed(rw_l.at[y], ry_send.at[0])
    landed(fin, ty_send.at[0])
    landed(rows.at[:, xcols(x)], tx_send.at[0])
    landed(hid.at[x], h_send.at[0])
    landed(dcross.at[:, mine], c_send.at[0])
    landed(dcross.at[:, mine], c_send.at[1])
    landed(ry_l, y_send.at[0])
    landed(fin.at[:, pl.ds(0, GROUPS - 1)], z_send.at[0])


def finish(n_z, n_y, land, dland, dcross, ret, spot, gate_out, up_out, down_out, mixed_out, mixed, sem):
    x = place(n_z, n_y)[3]
    tok, half = ret.shape
    hb, piece = dcross.shape[1:]
    q = land.shape[3]
    copies = []

    def put(src, dst):
        cp = pltpu.make_async_copy(src, dst, sem.at[len(copies)])
        cp.start()
        copies.append(cp)

    for i, out in enumerate((gate_out, up_out)):
        for a in range(HALVES):
            put(land.at[a, i], out.at[0, :, pl.ds(a * q, q)])
    for h in range(HALVES):
        put(dland.at[h, pl.ds(pl.multiple_of(x * hb, hb), hb)],
            down_out.at[0, :, pl.ds(pl.multiple_of(x * half + h * piece, piece), piece)])
        put(dcross.at[h],
            down_out.at[0, :, pl.ds(pl.multiple_of((1 - x) * half + h * piece, piece), piece)])
    everyone = (lax.broadcasted_iota(jnp.int32, (tok, tok), 0) == spot[0:1, :]).astype(BF16)
    mixed[...] = lax.dot_general(
        everyone, ret[...], (((0,), (0,)), ((), ())), preferred_element_type=jnp.float32).astype(BF16)
    put(mixed, mixed_out)
    for cp in copies:
        cp.wait()


def paired(n_z, n_y, tokens, route_ids, route_weights, norm_gain, gate_weight, up_weight, down_weight):
    tok, width = tokens.shape
    cap = tok // GROUPS
    half = width // lax.axis_size("tp")
    n_fs = n_z * n_y
    d_rows, d_cols = down_weight.shape[1:]
    g_rows, g_cols = gate_weight.shape[1:]
    f32, i32 = jnp.float32, jnp.int32
    q, piece = g_cols // HALVES, half // HALVES
    hb = n_fs * d_rows

    hbm = pl.BlockSpec(memory_space=pltpu.HBM)
    vmem = pl.BlockSpec(memory_space=pltpu.VMEM)
    dma = pltpu.SemaphoreType.DMA
    lanes = -(-cap // 128) * 128
    held = pl.pallas_call(
        functools.partial(sampler, n_z, n_y),
        out_shape=(
            pltpu.VMEM((HALVES, 2, 2 * n_fs * g_rows, q), BF16),
            pltpu.VMEM((HALVES, 2 * hb, piece), BF16),
            pltpu.VMEM((HALVES, hb, piece), BF16),
            pltpu.VMEM((tok, half), BF16),
            pltpu.VMEM((8, tok), i32),
        ),
        in_specs=[hbm] * 7,
        out_specs=(vmem,) * 5,
        scratch_shapes=[
            pltpu.VMEM((tok, width), BF16),
            pltpu.VMEM((2, tok), i32),
            pltpu.VMEM((2, tok), f32),
            pltpu.VMEM((1, g_rows), f32),
            pltpu.VMEM((n_fs, 2, g_rows, g_cols), f32),
            pltpu.VMEM((n_fs - 1, HALVES, 2, g_rows, q), BF16),
            pltpu.VMEM((n_fs, d_rows, d_cols), f32),
            pltpu.VMEM((HALVES, n_fs - 1, d_rows, piece), BF16),
            pltpu.VMEM((tok, half), BF16),
            pltpu.VMEM((3, cap, half), BF16),
            pltpu.VMEM((n_fs * cap, width), BF16),
            pltpu.VMEM((3, 8, lanes), f32),
            pltpu.VMEM((n_y, n_z, 8, lanes), f32),
            pltpu.VMEM((2, HALVES, n_fs * cap, q), BF16),
            pltpu.VMEM((HALVES, 4, 2, cap, piece), BF16),
            pltpu.VMEM((HALVES, 4, cap, piece), BF16),
            pltpu.VMEM((HALVES, 4, cap, piece), BF16),
            dma((4,)), dma((n_fs,)), dma((1,)),
            dma((2,)), dma((4, n_fs - 1)), dma((2,)), dma((4,)),
            dma((1,)), dma((3,)), dma((1,)), dma((4,)), dma((1,)), dma((1,)),
            dma((1,)), dma((3,)), dma((1,)), dma((1,)),
            dma((1,)), dma((HALVES, 4)), dma((2,)), dma((4,)),
            dma((1,)), dma((HALVES, 4)), dma((1,)), dma((2,)),
        ],
        compiler_params=pltpu.CompilerParams(
            collective_id=0, has_side_effects=True, vmem_limit_bytes=40 * 1024 * 1024),
    )(*(pltpu.with_memory_space_constraint(v, pltpu.HBM) for v in (
        tokens, route_ids.T, route_weights.T, norm_gain.reshape(1, g_rows),
        gate_weight, up_weight, down_weight)))
    return pl.pallas_call(
        functools.partial(finish, n_z, n_y),
        out_shape=(
            jax.ShapeDtypeStruct((1, 2 * n_fs * g_rows, g_cols), BF16),
            jax.ShapeDtypeStruct((1, 2 * n_fs * g_rows, g_cols), BF16),
            jax.ShapeDtypeStruct((1, hb, 2 * d_cols), BF16),
            jax.ShapeDtypeStruct((tok, half), BF16),
        ),
        in_specs=[vmem] * 5,
        out_specs=(hbm,) * 4,
        scratch_shapes=[pltpu.VMEM((tok, half), BF16), dma((9,))],
        compiler_params=pltpu.CompilerParams(vmem_limit_bytes=8 * 1024 * 1024),
    )(*(pltpu.with_memory_space_constraint(v, pltpu.VMEM) for v in held))


def solution(mesh):
    placed = (
        P(("gr", "fs"), None),
        P(("gr", "fs"), None),
        P(("gr", "fs"), None),
        P(("gr", "fs")),
        P(None, ("gr", "fs"), "tp"),
        P(None, ("gr", "fs"), "tp"),
        P(None, ("gr", "fs"), "tp"),
    )
    n_fs = mesh.shape["fs"]

    def body(*args):
        experts = args[4].shape[0]
        if experts == n_fs == 2 * GROUPS and mesh.shape["gr"] == mesh.shape["tp"] == 2:
            return paired(GROUPS, 2, *args)
        return local(*args)

    return jax.shard_map(
        body,
        mesh=mesh,
        in_specs=placed,
        out_specs=(
            P("fs", None, "tp"),
            P("fs", None, "tp"),
            P("fs", "tp", None),
            P(("gr", "fs"), "tp"),
        ),
        check_vma=False,
    )
```

time: 127 us -> 125 us (0.984)
  local copies, waits for them, and re-layouts: 8.26 us -> 0 us
  Pallas kernels: 118 us -> 124 us
    unnamed x12 -> x0, local copies, waits for them, and re-layouts: 8.26 us -> none
    pallas_call x1 -> x2, Pallas kernels: 118 us -> 124 us  [the longest x1 121 us: paired(): pl.pallas_call(functools.partial(sampler, n_z, n_y), out_shape=(pltpu.VME...]
where the time goes in v1:
time: 125 us
  Pallas kernels  124 us (99%)
    pallas_call x1, Pallas kernels, paired(): pl.pallas_call(functools.partial(sampler, n_z, n_y), out_shape=(pltpu.VME...  121 us
    pallas_call x1, Pallas kernels, paired(): pl.pallas_call(functools.partial(finish, n_z, n_y), out_shape=(jax.ShapeD...  2.97 us

profile of v1, /device:TPU:0, one launch (start us, length us, event | category | flops | bytes accessed | tf_op | source)
XLA Modules:
  0.0 124.7 jit_solution(7247810076126042429)
XLA Ops:
  0.6 121.0 %shard_map.102 = (bf16[2,2,2048,256]{3,2,1,0:T(8,128)(2,1)S(1)}, bf16[2,1024,512]{2,1,0:T(8,128)(2,1)S(1)}, bf16[2,512,512]{2,1,0:T(8,128)(2,1)S(1)}, bf16[384,1024]{1,0:T(8,128)(2,1)S(1)}, s32[8,384]{1,0:T(8,128)S(1)}) custom-call(bf16[384,2048]{1,0:T(8,128)(2,1)} %tok_hbm.1, s32[2,384]{1,0:T(2,128)} %bitcast.3, f32[2,384]{1,0:T(2,128)} %bitcast.4, ...), custom_call_target="tpu_custom_call" | custom-call | tf_op jit(solution)/shard_map/pallas_call | solution.py:467
  121.7 3.0 %shard_map.103 = (bf16[1,2048,512]{2,1,0:T(8,128)(2,1)}, bf16[1,2048,512]{2,1,0:T(8,128)(2,1)}, bf16[1,512,2048]{2,1,0:T(8,128)(2,1)}, bf16[384,1024]{1,0:T(8,128)(2,1)}) custom-call(bf16[2,2,2048,256]{3,2,1,0:T(8,128)(2,1)S(1)} %get-tuple-element.9.land, bf16[2,1024,512]{2,1,0:T(8,128)(2,1)S(1)} %get-tuple-element.10.dland, ...), custom_call_target="tpu_custom_call" | custom-call | tf_op jit(solution)/shard_map/pallas_call | solution.py:508

commit v2 on v1

--- a/solution.py
+++ b/solution.py
@@ -124,11 +124,12 @@
     piece = half // HALVES
     f32 = jnp.float32
     dev = functools.partial(device, n_y=n_y)
-    ks = [(kz, 0) for kz in (3, 2, 1)] + [(kz, 1) for kz in (3, 2, 1, 0)] + [(0, 0)]
+    ks = [(kz, ky) for kz in (3, 2, 1) for ky in (0, 1)] + [(0, 1), (0, 0)]
     last = len(ks) - 1
     at = []
     for kz, ky in ks:
-        pz, py = flip(z, kz), (1 - y if ky else y)
+        pz = flip(z, kz)
+        py = lax.rem(y + ky + c, 2) if kz else (1 - y if ky else y)
         at.append((pz * n_y + py, dev(c, pz, py, x)))
     other = dev(1 - c, z, y, x)
     x_nbr = dev(c, z, y, 1 - x)
@@ -360,13 +361,17 @@
         else:
             ret[trow(z), d] = total
 
-    for h in range(HALVES):
+    def collect(h):
         for n in order:
             arrive[n, 2 + h].wait_recv()
             dforward(n, h)
+
+    def project(h):
         landed(dland.at[h, core_rows(1 - c, d_rows)], f_recv.at[2 + h])
         cp = remote(dland.at[h, pl.ds(pl.multiple_of((1 - x) * hb + c * part, part), part)],
                     dcross.at[h, mine], c_send.at[0], c_recv.at[h], x_nbr)
+        cp.start()
+        cross.append(cp)
         for n, kz in enumerate(RETURN):
             zs = flip(z, kz)
             if h == 0:
@@ -388,11 +393,15 @@
                     ysend[n, h] = remote(out_s.at[h, n, 0], ry_l.at[h, n],
                                          y_send.at[0], y_recv.at[h, n], y_nbr)
                     ysend[n, h].start()
-            if n:
-                give_back(n - 1, h)
-        cp.start()
-        cross.append(cp)
-        give_back(len(RETURN) - 1, h)
+
+    collect(0)
+    project(0)
+    collect(1)
+    for n in range(len(RETURN)):
+        give_back(n, 0)
+    project(1)
+    for n in range(len(RETURN)):
+        give_back(n, 1)
 
     over = []
     for h in range(HALVES):

time: 125 us -> 117 us (0.936)
  Pallas kernels: 124 us -> 116 us
    pallas_call x1, Pallas kernels: 121 us -> 113 us  [paired(): pl.pallas_call(functools.partial(sampler, n_z, n_y), out_shape=(pltpu.VME...]
where the time goes in v2:
time: 117 us; the launch traced here: 116 us
  Pallas kernels  116 us (99%)
    pallas_call x1, Pallas kernels, paired(): pl.pallas_call(functools.partial(sampler, n_z, n_y), out_shape=(pltpu.VME...  113 us
    pallas_call x1, Pallas kernels, paired(): pl.pallas_call(functools.partial(finish, n_z, n_y), out_shape=(jax.ShapeD...  2.97 us

profile of v2, /device:TPU:0, one launch (start us, length us, event | category | flops | bytes accessed | tf_op | source)
XLA Modules:
  0.0 116.5 jit_solution(18126393839925261014)
XLA Ops:
  0.6 112.8 %shard_map.102 = (bf16[2,2,2048,256]{3,2,1,0:T(8,128)(2,1)S(1)}, bf16[2,1024,512]{2,1,0:T(8,128)(2,1)S(1)}, bf16[2,512,512]{2,1,0:T(8,128)(2,1)S(1)}, bf16[384,1024]{1,0:T(8,128)(2,1)S(1)}, s32[8,384]{1,0:T(8,128)S(1)}) custom-call(bf16[384,2048]{1,0:T(8,128)(2,1)} %tok_hbm.1, s32[2,384]{1,0:T(2,128)} %bitcast.3, f32[2,384]{1,0:T(2,128)} %bitcast.4, ...), custom_call_target="tpu_custom_call" | custom-call | tf_op jit(solution)/shard_map/pallas_call | solution.py:476
  113.5 3.0 %shard_map.103 = (bf16[1,2048,512]{2,1,0:T(8,128)(2,1)}, bf16[1,2048,512]{2,1,0:T(8,128)(2,1)}, bf16[1,512,2048]{2,1,0:T(8,128)(2,1)}, bf16[384,1024]{1,0:T(8,128)(2,1)}) custom-call(bf16[2,2,2048,256]{3,2,1,0:T(8,128)(2,1)S(1)} %get-tuple-element.9.land, bf16[2,1024,512]{2,1,0:T(8,128)(2,1)S(1)} %get-tuple-element.10.dland, ...), custom_call_target="tpu_custom_call" | custom-call | tf_op jit(solution)/shard_map/pallas_call | solution.py:517

commit v3 on v2

--- a/solution.py
+++ b/solution.py
@@ -76,18 +76,14 @@
 
 
 def flip(z, k):
-    return (z, z + 1 - 2 * lax.rem(z, 2), lax.rem(z + 2, 4), 3 - z)[k]
+    steps = (z, z + 1 - 2 * lax.rem(z, 2), lax.rem(z + 2, 4), 3 - z)
+    if isinstance(k, int):
+        return steps[k]
+    return jnp.where(k == 1, steps[1], jnp.where(k == 2, steps[2], steps[3]))
 
 
 def device(c, z, y, x, n_y):
     return {"gr": c, "fs": z * n_y + y, "tp": x}
-
-
-def greet(peers):
-    barrier = pltpu.get_barrier_semaphore()
-    for peer in peers:
-        pl.semaphore_signal(barrier, inc=1, device_id=peer, device_id_type=MESH)
-    return lambda: pl.semaphore_wait(barrier, len(peers))
 
 
 def remote(src, dst, send, recv, peer):
@@ -107,7 +103,7 @@
     land, dland, dcross, ret, spot,
     tok_in, ids_in, rw_in, gain_in, wide, narrow, dwide, dnarrow,
     normed, tok_s, rows, rw_s, rw_l, hid, out_s, ry_l, fin,
-    in_sem, ld_sem, dl_sem, w_send, w_recv, f_send, f_recv,
+    ready, in_sem, ld_sem, dl_sem, w_send, w_recv, f_send, f_recv,
     tz_send, tz_recv, ty_send, ty_recv, tx_send, tx_recv,
     rz_send, rz_recv, ry_send, ry_recv,
     h_send, h_recv, c_send, c_recv, y_send, y_recv, z_send, z_recv,
@@ -124,13 +120,18 @@
     piece = half // HALVES
     f32 = jnp.float32
     dev = functools.partial(device, n_y=n_y)
-    ks = [(kz, ky) for kz in (3, 2, 1) for ky in (0, 1)] + [(0, 1), (0, 0)]
-    last = len(ks) - 1
-    at = []
-    for kz, ky in ks:
+    outer = (z == 0) | (z == n_z - 1)
+    near, far = jnp.where(outer, 1, 3), jnp.where(outer, 3, 1)
+    last = n_fs - 1
+
+    def partner(kz, ky):
         pz = flip(z, kz)
-        py = lax.rem(y + ky + c, 2) if kz else (1 - y if ky else y)
-        at.append((pz * n_y + py, dev(c, pz, py, x)))
+        py = 1 - y if isinstance(kz, int) and kz == 0 else lax.rem(y + ky + c, 2)
+        return pz * n_y + py, dev(c, pz, py, x), kz
+
+    at = [partner(kz, ky) for kz in (near, far, 2) for ky in range(2)]
+    at += [partner(0, 1), (me, None, None)]
+    peers = [partner(kz, ky) for kz in (1, 2, 3) for ky in range(2)] + [partner(0, 1)]
     other = dev(1 - c, z, y, x)
     x_nbr = dev(c, z, y, 1 - x)
     y_nbr = dev(c, z, 1 - y, x)
@@ -150,7 +151,29 @@
     def trow(f):
         return pl.ds(pl.multiple_of(f * cap, cap), cap)
 
-    met = greet([d for _, d in at[:last]] + [other, x_nbr])
+    barrier = pltpu.get_barrier_semaphore()
+
+    def tell(sem, peer):
+        pl.semaphore_signal(sem, inc=1, device_id=peer, device_id_type=MESH)
+
+    beside = [peers[k][1] for k in (4, 5, 6)] + [other, x_nbr]
+    across = [peers[k][1] for k in range(4)]
+    for peer in beside:
+        tell(barrier, peer)
+
+    @pl.when(jnp.logical_not(outer))
+    def _():
+        for peer in across:
+            tell(barrier, peer)
+
+    def met():
+        pl.semaphore_wait(barrier, len(beside) + jnp.where(outer, len(across), 0))
+
+        @pl.when(outer)
+        def _():
+            for peer in across:
+                tell(ready, peer)
+
     small = []
 
     def fetch(src, dst):
@@ -163,17 +186,13 @@
 
     def load(n):
         for i, ref in enumerate((gate_in, up_in)):
-            pltpu.make_async_copy(ref.at[at[n][0]], wide.at[n, i], ld_sem.at[n]).start()
+            pltpu.make_async_copy(ref.at[at[n][0]], wide.at[n, i], ld_sem.at[int(n >= HEAD)]).start()
 
     for n in range(HEAD):
         load(n)
     fetch(tok_hbm, tok_in)
     fetch(ids_hbm, ids_in)
     fetch(rw_hbm, rw_in)
-    for n in range(HEAD, last + 1):
-        load(n)
-    for n, (p, _) in enumerate(at):
-        pltpu.make_async_copy(down_in.at[p], dwide.at[n], dl_sem.at[0]).start()
 
     def column(row, count):
         lanes = row.shape[1]
@@ -185,7 +204,6 @@
     gain = column(gain_in[...], g_rows)
 
     def fold(n):
-        landed(wide.at[n], ld_sem.at[n])
         for i in range(2):
             value = (wide[n, i] * gain).astype(BF16)
             for a in range(HALVES):
@@ -195,27 +213,33 @@
                 else:
                     narrow[n, a, i] = part
 
-    arrive = {}
-    onward = {}
-
-    def forward(n, a):
-        block = land.at[a, :, grow(c, at[n][0]), :]
-        onward[n, a] = remote(block, block, f_send.at[0], f_recv.at[a], other)
-        onward[n, a].start()
+    def forward(f, a):
+        block = land.at[a, :, grow(c, f), :]
+        remote(block, block, f_send.at[0], f_recv.at[a], other).start()
+
+    def arrived(kz, a):
+        group = [f for f, _, k in peers if k == kz]
+        landed(narrow.at[pl.ds(0, len(group)), a], w_recv.at[a, kz])
+        for f in group:
+            forward(f, a)
 
     def spread(n, a):
         if n == last:
-            forward(n, a)
+            forward(me, a)
         else:
-            arrive[n, a] = remote(narrow.at[n, a], land.at[a, :, grow(c, me), :],
-                                  w_send.at[0], w_recv.at[a, n], at[n][1])
-            arrive[n, a].start()
-
+            remote(narrow.at[n, a], land.at[a, :, grow(c, me), :],
+                   w_send.at[0], w_recv.at[a, at[n][2]], at[n][1]).start()
+
+    landed(wide.at[pl.ds(0, HEAD)], ld_sem.at[0])
     for n in range(HEAD):
         fold(n)
     met()
     for n in range(HEAD):
         spread(n, 0)
+    for n in range(HEAD, last + 1):
+        load(n)
+    for n, (p, _, _) in enumerate(at):
+        pltpu.make_async_copy(down_in.at[p], dwide.at[n], dl_sem.at[0]).start()
 
     for cp in small[1:]:
         cp.wait()
@@ -249,7 +273,12 @@
     def picked(g):
         return lax.broadcasted_iota(jnp.int32, (cap, tok), 0) + g * cap == position
 
-    tz, rz, ty, tx, ry = {}, {}, {}, {}, {}
+    def hop(kz):
+        peer = dev(c, flip(z, kz), y, x)
+        return (remote(tok_s.at[kz - 1], rows.at[trow(me), xcols(x)],
+                       tz_send.at[0], tz_recv.at[kz - 1], peer),
+                remote(rw_s.at[kz - 1], rw_l.at[y, z], rz_send.at[0], rz_recv.at[kz - 1], peer))
+
     for kz in (3, 2, 1, 0):
         g = flip(z, kz)
         pick = picked(g)
@@ -258,33 +287,41 @@
                                 precision=lax.Precision.HIGHEST, preferred_element_type=f32)
         if kz:
             tok_s[kz - 1] = block
-            rw_s[kz - 1, :, :cap] = w_row
-            peer = dev(c, g, y, x)
-            tz[kz] = remote(tok_s.at[kz - 1], rows.at[trow(me), xcols(x)],
-                            tz_send.at[0], tz_recv.at[kz - 1], peer)
-            tz[kz].start()
-            rz[kz] = remote(rw_s.at[kz - 1], rw_l.at[y, z], rz_send.at[0], rz_recv.at[kz - 1], peer)
-            rz[kz].start()
+            rw_s[kz - 1, :, :cap] = w_row[:2]
+            if kz == 2:
+                @pl.when(jnp.logical_not(outer))
+                def _():
+                    pl.semaphore_wait(ready, len(across))
+            for cp in hop(kz):
+                cp.start()
         else:
             rows[trow(me), xcols(x)] = block
-            rw_l[y, z, :, :cap] = w_row
+            rw_l[y, z, :, :cap] = w_row[:2]
 
     def pass_x(f):
         block = rows.at[trow(f), xcols(x)]
-        tx[len(tx)] = remote(block, block, tx_send.at[0], tx_recv.at[0], x_nbr)
-        tx[len(tx) - 1].start()
+        remote(block, block, tx_send.at[0], tx_recv.at[0], x_nbr).start()
 
     def pass_on(kz):
         zs = flip(z, kz)
         src = zs * n_y + y
         block = rows.at[trow(src), xcols(x)]
-        ty[kz] = remote(block, block, ty_send.at[0], ty_recv.at[kz], y_nbr)
-        ty[kz].start()
+        remote(block, block, ty_send.at[0], ty_recv.at[kz], y_nbr).start()
         pass_x(src)
-        ry[kz] = remote(rw_l.at[y, zs], rw_l.at[y, zs], ry_send.at[0], ry_recv.at[0], y_nbr)
-        ry[kz].start()
+        remote(rw_l.at[y, zs], rw_l.at[y, zs], ry_send.at[0], ry_recv.at[0], y_nbr).start()
+
+    def from_z(kz):
+        for cp in hop(kz):
+            cp.wait_recv()
+        pass_on(kz)
+
+    def from_y(kz):
+        f = flip(z, kz) * n_y + 1 - y
+        landed(rows.at[trow(f), xcols(x)], ty_recv.at[kz])
+        pass_x(f)
 
     pass_on(0)
+    landed(wide.at[pl.ds(HEAD, n_fs - HEAD)], ld_sem.at[1])
     for n in range(HEAD, last + 1):
         fold(n)
         spread(n, 0)
@@ -292,38 +329,41 @@
         spread(n, 1)
 
     landed(dwide, dl_sem.at[0])
-
-    def dforward(n, h):
-        block = dland.at[h, drow(c, at[n][0])]
-        onward[n, 2 + h] = remote(block, block, f_send.at[1], f_recv.at[2 + h], other)
-        onward[n, 2 + h].start()
-
     for h in range(HALVES):
         for n in range(last + 1):
             value = dwide[n, :, h * piece:(h + 1) * piece].astype(BF16)
             if n == last:
                 dland[h, drow(c, me)] = value
-                dforward(n, h)
             else:
                 dnarrow[h, n] = value
-                arrive[n, 2 + h] = remote(dnarrow.at[h, n], dland.at[h, drow(c, me)],
-                                          w_send.at[1], w_recv.at[2 + h, n], at[n][1])
-                arrive[n, 2 + h].start()
-
-    for kz in (1, 3, 2):
-        tz[kz].wait_recv()
-        rz[kz].wait_recv()
-        pass_on(kz)
-    for kz in (0, 1, 3, 2):
-        ty[kz].wait_recv()
-        pass_x(flip(z, kz) * n_y + 1 - y)
-
-    order = sorted(range(last), key=lambda n: ks[n])
+
+    def dforward(f, h):
+        block = dland.at[h, drow(c, f)]
+        remote(block, block, f_send.at[1], f_recv.at[2 + h], other).start()
+
+    def dspread():
+        for h in range(HALVES):
+            for n in range(last):
+                remote(dnarrow.at[h, n], dland.at[h, drow(c, me)],
+                       w_send.at[1], w_recv.at[2 + h, at[n][2]], at[n][1]).start()
+            dforward(me, h)
+
+    @pl.when(jnp.logical_not(outer))
+    def _():
+        dspread()
+
+    early, late = jnp.where(outer, 3, 2), jnp.where(outer, 2, 3)
+    from_z(early)
+    from_y(0)
+    from_z(1)
+    from_y(early)
+    from_y(1)
+    from_z(late)
+    from_y(late)
 
     def gather(a):
-        for n in order:
-            arrive[n, a].wait_recv()
-            forward(n, a)
+        for kz in range(n_z):
+            arrived(kz, a)
         if a == 0:
             landed(rows.at[:, xcols(1 - x)], tx_recv.at[0])
             landed(rw_l.at[1 - y], ry_recv.at[0])
@@ -333,6 +373,10 @@
     hsend = {}
     for a in range(HALVES):
         gather(a)
+        if a == 1:
+            @pl.when(outer)
+            def _():
+                dspread()
         for n, kz in enumerate(RETURN):
             r = pl.ds(pl.multiple_of(flip(z, kz) * m, m), m)
             v = jnp.dot(rows[r, :], land[a, 0], preferred_element_type=f32)
@@ -346,7 +390,6 @@
     mine = pl.ds(pl.multiple_of(c * part, part), part)
     cross = []
     ysend = {}
-    zsend = {}
 
     def give_back(n, h):
         kz = RETURN[n]
@@ -355,16 +398,17 @@
         d = pl.ds(h * piece, piece)
         if kz:
             fin[h, n] = total
-            zsend[n, h] = remote(fin.at[h, n], ret.at[trow(z), d], z_send.at[0], z_recv.at[h],
-                                 dev(c, flip(z, kz), y, x))
-            zsend[n, h].start()
+            remote(fin.at[h, n], ret.at[trow(z), d], z_send.at[0], z_recv.at[h],
+                   dev(c, flip(z, kz), y, x)).start()
         else:
             ret[trow(z), d] = total
 
     def collect(h):
-        for n in order:
-            arrive[n, 2 + h].wait_recv()
-            dforward(n, h)
+        for kz in range(n_z):
+            group = [f for f, _, k in peers if k == kz]
+            landed(dnarrow.at[h, pl.ds(0, len(group))], w_recv.at[2 + h, kz])
+            for f in group:
+                dforward(f, h)
 
     def project(h):
         landed(dland.at[h, core_rows(1 - c, d_rows)], f_recv.at[2 + h])
@@ -396,20 +440,35 @@
 
     collect(0)
     project(0)
+    @pl.when(jnp.logical_not(outer))
+    def _():
+        give_back(0, 0)
+        give_back(1, 0)
+
     collect(1)
-    for n in range(len(RETURN)):
-        give_back(n, 0)
+
+    @pl.when(outer)
+    def _():
+        give_back(0, 0)
+        give_back(1, 0)
+
     project(1)
-    for n in range(len(RETURN)):
-        give_back(n, 1)
-
     over = []
-    for h in range(HALVES):
+
+    def cross_on(h):
         cross[h].wait_recv()
         block = dcross.at[h, mine]
         cp = remote(block, block, c_send.at[1], c_recv.at[2 + h], other)
         cp.start()
         over.append(cp)
+
+    cross_on(0)
+    give_back(2, 0)
+    give_back(3, 0)
+    for n in range(len(RETURN)):
+        if n == 3:
+            cross_on(1)
+        give_back(n, 1)
     for h in range(HALVES):
         landed(fin.at[h, pl.ds(0, GROUPS - 1)], z_recv.at[h])
     for cp in over:
@@ -496,14 +555,14 @@
             pltpu.VMEM((tok, half), BF16),
             pltpu.VMEM((3, cap, half), BF16),
             pltpu.VMEM((n_fs * cap, width), BF16),
-            pltpu.VMEM((3, 8, lanes), f32),
-            pltpu.VMEM((n_y, n_z, 8, lanes), f32),
+            pltpu.VMEM((3, 2, lanes), f32),
+            pltpu.VMEM((n_y, n_z, 2, lanes), f32),
             pltpu.VMEM((2, HALVES, n_fs * cap, q), BF16),
             pltpu.VMEM((HALVES, 4, 2, cap, piece), BF16),
             pltpu.VMEM((HALVES, 4, cap, piece), BF16),
             pltpu.VMEM((HALVES, 4, cap, piece), BF16),
-            dma((4,)), dma((n_fs,)), dma((1,)),
-            dma((2,)), dma((4, n_fs - 1)), dma((2,)), dma((4,)),
+            pltpu.SemaphoreType.REGULAR, dma((4,)), dma((2,)), dma((1,)),
+            dma((2,)), dma((4, 4)), dma((2,)), dma((4,)),
             dma((1,)), dma((3,)), dma((1,)), dma((4,)), dma((1,)), dma((1,)),
             dma((1,)), dma((3,)), dma((1,)), dma((1,)),
             dma((1,)), dma((HALVES, 4)), dma((2,)), dma((4,)),

time: 117 us -> 112 us (0.957)
  Pallas kernels: 116 us -> 111 us
    pallas_call x1, Pallas kernels: 113 us -> 108 us  [paired(): pl.pallas_call(functools.partial(sampler, n_z, n_y), out_shape=(pltpu.VME...]
where the time goes in v3:
time: 112 us
  Pallas kernels  111 us (99%)
    pallas_call x1, Pallas kernels, paired(): pl.pallas_call(functools.partial(sampler, n_z, n_y), out_shape=(pltpu.VME...  108 us
    pallas_call x1, Pallas kernels, paired(): pl.pallas_call(functools.partial(finish, n_z, n_y), out_shape=(jax.ShapeD...  2.97 us

profile of v3, /device:TPU:0, one launch (start us, length us, event | category | flops | bytes accessed | tf_op | source)
XLA Modules:
  0.0 111.8 jit_solution(4145359850140316104)
XLA Ops:
  0.6 108.2 %shard_map.102 = (bf16[2,2,2048,256]{3,2,1,0:T(8,128)(2,1)S(1)}, bf16[2,1024,512]{2,1,0:T(8,128)(2,1)S(1)}, bf16[2,512,512]{2,1,0:T(8,128)(2,1)S(1)}, bf16[384,1024]{1,0:T(8,128)(2,1)S(1)}, s32[8,384]{1,0:T(8,128)S(1)}) custom-call(bf16[384,2048]{1,0:T(8,128)(2,1)} %tok_hbm.1, s32[2,384]{1,0:T(2,128)} %bitcast.3, f32[2,384]{1,0:T(2,128)} %bitcast.4, ...), custom_call_target="tpu_custom_call" | custom-call | tf_op jit(solution)/shard_map/pallas_call | solution.py:535
  108.8 3.0 %shard_map.103 = (bf16[1,2048,512]{2,1,0:T(8,128)(2,1)}, bf16[1,2048,512]{2,1,0:T(8,128)(2,1)}, bf16[1,512,2048]{2,1,0:T(8,128)(2,1)}, bf16[384,1024]{1,0:T(8,128)(2,1)}) custom-call(bf16[2,2,2048,256]{3,2,1,0:T(8,128)(2,1)S(1)} %get-tuple-element.9.land, bf16[2,1024,512]{2,1,0:T(8,128)(2,1)S(1)} %get-tuple-element.10.dland, ...), custom_call_target="tpu_custom_call" | custom-call | tf_op jit(solution)/shard_map/pallas_call | solution.py:576

commit v4 on v3

--- a/solution.py
+++ b/solution.py
@@ -10,7 +10,6 @@
 GROUPS = 4
 HEAD = 2
 HALVES = 2
-RETURN = (3, 2, 1, 0)
 BF16 = jnp.bfloat16
 MESH = pl.DeviceIdType.MESH
 
@@ -151,6 +150,21 @@
     def trow(f):
         return pl.ds(pl.multiple_of(f * cap, cap), cap)
 
+    small = []
+
+    def fetch(src, dst):
+        cp = pltpu.make_async_copy(src, dst, in_sem.at[len(small)])
+        cp.start()
+        small.append(cp)
+
+    fetch(gain_hbm, gain_in)
+
+    def load(n):
+        for i, ref in enumerate((gate_in, up_in)):
+            pltpu.make_async_copy(ref.at[at[n][0]], wide.at[n, i], ld_sem.at[int(n >= HEAD)]).start()
+
+    for n in range(HEAD):
+        load(n)
     barrier = pltpu.get_barrier_semaphore()
 
     def tell(sem, peer):
@@ -166,6 +180,10 @@
         for peer in across:
             tell(barrier, peer)
 
+    fetch(tok_hbm, tok_in)
+    fetch(ids_hbm, ids_in)
+    fetch(rw_hbm, rw_in)
+
     def met():
         pl.semaphore_wait(barrier, len(beside) + jnp.where(outer, len(across), 0))
 
@@ -173,26 +191,6 @@
         def _():
             for peer in across:
                 tell(ready, peer)
-
-    small = []
-
-    def fetch(src, dst):
-        cp = pltpu.make_async_copy(src, dst, in_sem.at[len(small)])
-        cp.start()
-        small.append(cp)
-
-    fetch(gain_hbm, gain_in)
-    loads = {}
-
-    def load(n):
-        for i, ref in enumerate((gate_in, up_in)):
-            pltpu.make_async_copy(ref.at[at[n][0]], wide.at[n, i], ld_sem.at[int(n >= HEAD)]).start()
-
-    for n in range(HEAD):
-        load(n)
-    fetch(tok_hbm, tok_in)
-    fetch(ids_hbm, ids_in)
-    fetch(rw_hbm, rw_in)
 
     def column(row, count):
         lanes = row.shape[1]
@@ -370,6 +368,7 @@
         landed(land.at[a, :, core_rows(1 - c, g_rows), :], f_recv.at[a])
 
     m = n_y * cap
+    back = (early, late, 1, 0)
     hsend = {}
     for a in range(HALVES):
         gather(a)
@@ -377,7 +376,7 @@
             @pl.when(outer)
             def _():
                 dspread()
-        for n, kz in enumerate(RETURN):
+        for n, kz in enumerate(back):
             r = pl.ds(pl.multiple_of(flip(z, kz) * m, m), m)
             v = jnp.dot(rows[r, :], land[a, 0], preferred_element_type=f32)
             w = jnp.dot(rows[r, :], land[a, 1], preferred_element_type=f32)
@@ -392,11 +391,11 @@
     ysend = {}
 
     def give_back(n, h):
-        kz = RETURN[n]
+        kz = back[n]
         ysend[n, h].wait_recv()
         total = (out_s[h, n, 1].astype(f32) + ry_l[h, n].astype(f32)).astype(BF16)
         d = pl.ds(h * piece, piece)
-        if kz:
+        if n < 3:
             fin[h, n] = total
             remote(fin.at[h, n], ret.at[trow(z), d], z_send.at[0], z_recv.at[h],
                    dev(c, flip(z, kz), y, x)).start()
@@ -416,7 +415,7 @@
                     dcross.at[h, mine], c_send.at[0], c_recv.at[h], x_nbr)
         cp.start()
         cross.append(cp)
-        for n, kz in enumerate(RETURN):
+        for n, kz in enumerate(back):
             zs = flip(z, kz)
             if h == 0:
                 for a in range(HALVES):
@@ -465,7 +464,7 @@
     cross_on(0)
     give_back(2, 0)
     give_back(3, 0)
-    for n in range(len(RETURN)):
+    for n in range(len(back)):
         if n == 3:
             cross_on(1)
         give_back(n, 1)

time: 112 us -> 111 us (level)
  Pallas kernels: 111 us -> 109 us
    pallas_call x1, Pallas kernels: 108 us -> 106 us  [paired(): pl.pallas_call(functools.partial(sampler, n_z, n_y), out_shape=(pltpu.VME...]
where the time goes in v4:
time: 111 us; the launch traced here: 110 us
  Pallas kernels  109 us (98%)
    pallas_call x1, Pallas kernels, paired(): pl.pallas_call(functools.partial(sampler, n_z, n_y), out_shape=(pltpu.VME...  106 us
    pallas_call x1, Pallas kernels, paired(): pl.pallas_call(functools.partial(finish, n_z, n_y), out_shape=(jax.ShapeD...  2.97 us

profile of v4, /device:TPU:0, one launch (start us, length us, event | category | flops | bytes accessed | tf_op | source)
XLA Modules:
  0.0 109.8 jit_solution(876050860106381578)
XLA Ops:
  0.6 106.2 %shard_map.102 = (bf16[2,2,2048,256]{3,2,1,0:T(8,128)(2,1)S(1)}, bf16[2,1024,512]{2,1,0:T(8,128)(2,1)S(1)}, bf16[2,512,512]{2,1,0:T(8,128)(2,1)S(1)}, bf16[384,1024]{1,0:T(8,128)(2,1)S(1)}, s32[8,384]{1,0:T(8,128)S(1)}) custom-call(bf16[384,2048]{1,0:T(8,128)(2,1)} %tok_hbm.1, s32[2,384]{1,0:T(2,128)} %bitcast.3, f32[2,384]{1,0:T(2,128)} %bitcast.4, ...), custom_call_target="tpu_custom_call" | custom-call | tf_op jit(solution)/shard_map/pallas_call | solution.py:534
  106.8 3.0 %shard_map.103 = (bf16[1,2048,512]{2,1,0:T(8,128)(2,1)}, bf16[1,2048,512]{2,1,0:T(8,128)(2,1)}, bf16[1,512,2048]{2,1,0:T(8,128)(2,1)}, bf16[384,1024]{1,0:T(8,128)(2,1)}) custom-call(bf16[2,2,2048,256]{3,2,1,0:T(8,128)(2,1)S(1)} %get-tuple-element.9.land, bf16[2,1024,512]{2,1,0:T(8,128)(2,1)S(1)} %get-tuple-element.10.dland, ...), custom_call_target="tpu_custom_call" | custom-call | tf_op jit(solution)/shard_map/pallas_call | solution.py:575
